TPU v7x, 512 devices: a whole 4x8x8 slice. The times are simulated.
512 devices in a mesh: ep: 32 (over z, x), tp: 16 (over y, core).
Axes of the slice: x: 4, y: 8, z: 8, core: 2. Of those that a mesh axis runs over, the one named last changes fastest.
Arguments:
- blender_incoming_features: bfloat16 [8192, 4096], P('ep', 'tp'), may hold values from -6 to 6
- entry_latent_matrix: bfloat16 [8192, 2048], P('ep', 'tp'), may hold values from -6 to 6
- exit_latent_matrix: bfloat16 [8192, 2048], P('ep', 'tp'), may hold values from -6 to 6
- unactivated_valve: bfloat16 [8192, 4096], P('ep', 'tp'), may hold values from -6 to 6
- presoftplus_strides: float32 [8192, 64], P('ep', 'tp'), may hold values from -7 to 7
- extra_attenuation: float32 [8192, 64], P('ep', 'tp'), may hold values from -1 to 0
- incoming_feature_kernel: bfloat16 [4, 4096], P(None, 'tp'), may hold values from -3 to 3
- entry_latent_kernel: bfloat16 [4, 2048], P(None, 'tp'), may hold values from -3 to 3
- exit_latent_kernel: bfloat16 [4, 2048], P(None, 'tp'), may hold values from -3 to 3
- stride_offset_vector: float32 [64], P('tp'), may hold values from -1 to 1
- attenuation_speed_exponent: float32 [64], P('tp'), may hold values from -16 to -3
- bypass_coef_vector: float32 [64], P('tp'), may hold values from 0.5 to 4
- cluster_rescale_coefs: bfloat16 [4096], P('tp'), may hold values from 0.099609375 to 1.8984375
- blender_result_matrix: bfloat16 [4096, 2048], P('tp'), may hold values from -0.09375 to 0.09375
- latter_microbatch_activations: bfloat16 [8192, 2048], P('ep'), may hold values from -6 to 6
- specialist_rescale_coefs: bfloat16 [2048], replicated, may hold values from 0.099609375 to 1.8984375
- specialist_valve_matrix: bfloat16 [32, 2048, 4096], P('ep', None, 'tp'), may hold values from -0.125 to 0.125
- specialist_expand_matrix: bfloat16 [32, 2048, 4096], P('ep', None, 'tp'), may hold values from -0.125 to 0.125
- specialist_contract_matrix: bfloat16 [32, 4096, 2048], P('ep', 'tp'), may hold values from -0.125 to 0.125
- specialist_picks: int32 [8192, 2], P('ep'), may hold values from 0 to 31, all different within a row; in each aligned block of 256 rows (0 to 255, 256 to 511, ...) at most 24 rows name the same one
- selected_specialist_coefs: float32 [8192, 2], P('ep'), may hold values from 0.1 to 1
Outputs:
- mixed_a: bfloat16 [8192, 2048], P(('ep', 'tp'))
- mixed_b: bfloat16 [8192, 2048], P('ep', 'tp')
Inputs may be any that keep to these rules, and one draw needn't show every extreme that they name: `specialist_picks`: in each aligned block of 256 rows, the rows of one index of ep, no expert is named by more than 24 rows, a bound that some block reaches.
All inputs are finite; a program needn't handle non-finite values.
Results may differ from a plain program's by a relative error of at most 0.019.
Values may be sent and summed in bfloat16 or wider, within the bound.
No kernel may reach another device: no remote copies, remote signals or barrier semaphores. Data moves between devices by JAX's collectives and lax.ppermute only.
A program may use at most 64 MiB of HBM per device.

v0:
```python
import jax
import jax.numpy as jnp
from jax import lax
from jax.sharding import Mesh
from jax.sharding import PartitionSpec as P

HEADS = 64
HEAD_DIM = 64
SHARING_CLUSTERS = 16
STATE = 128
BLOCK = 64
TOPK = 2
EP = ("ep_0", "ep_1")
TP = ("tp_0", "tp_1")
EP_TP = ("ep_0", "ep_1", "tp_0", "tp_1")
NORM_EPS = 1e-06


def from_behind(block, axis, distance):
    devices = range(lax.axis_size(axis))
    route = [(i - distance, i) for i in devices if i - distance in devices]
    return lax.ppermute(block, axis, route)


def filled_with(x, identity):
    return jax.tree.map(
        lambda part, zero: jnp.zeros_like(part) + jnp.asarray(zero, part.dtype), x, identity
    )


def carried_in(x, axes, combine, identity):
    before = start = filled_with(x, identity)
    running = x
    for axis in reversed(axes):
        count, place = (lax.axis_size(axis), lax.axis_index(axis))
        pieces = jax.tree.map(
            lambda part, kind: lax.all_gather(part.astype(kind), axis),
            running,
            (jnp.bfloat16, jnp.bfloat16),
        )
        inside, running = (start, start)
        for k in range(count):
            passed = k < place
            running = combine(
                running, jax.tree.map(lambda part, own: part[k].astype(own.dtype), pieces, x)
            )
            inside = jax.tree.map(lambda new, old: jnp.where(passed, new, old), running, inside)
        before = combine(inside, before)
    return before


def in_blocks(x, dim, count):
    before, after = (x.shape[:dim], x.shape[dim + 1 :])
    return jnp.moveaxis(x.reshape(*before, count, -1, *after), dim, 0)


def summed_on_arrival(x, axis, dim):
    tiles = in_blocks(x, dim, lax.axis_size(axis))
    arrived = lax.all_to_all(tiles, axis, split_axis=0, concat_axis=0, tiled=True)
    return arrived.astype(jnp.float32).sum(axis=0)


def summed_rows(x, axes, dim):
    for axis in axes:
        x = lax.psum_scatter(x, axis, scatter_dimension=dim, tiled=True)
    return x


def conv_silu(inputs, rim_rows, weight):
    tap_count = weight.shape[0]
    context_span = inputs.shape[0]
    joined = jnp.concatenate([rim_rows, inputs], axis=0).astype(jnp.float32)
    kernel = weight.astype(jnp.float32)
    running_total = kernel[0] * joined[0:context_span]
    for offset in range(1, tap_count):
        running_total = running_total + kernel[offset] * joined[offset : offset + context_span]
    return jax.nn.silu(running_total)


def block_step(carry_state, inputs):
    scaled_x, b_block, c_block, log_block = inputs
    context_span = log_block.shape[0]
    running = jnp.cumsum(log_block, axis=0)
    causal = (jnp.arange(context_span)[:, None] >= jnp.arange(context_span)[None, :])[
        :, :, None, None
    ]
    log_gap = running[:, None] - running[None, :]
    weights = jnp.where(causal, jnp.exp(jnp.where(causal, log_gap, 0.0)), 0.0)
    scores = jnp.einsum("lgn,sgn->lsg", c_block, b_block, preferred_element_type=jnp.float32)
    inside = jnp.einsum("lsgj,sgjp->lgjp", scores[..., None] * weights, scaled_x)
    c_wide = c_block.astype(jnp.float32)
    b_wide = b_block.astype(jnp.float32)
    before = jnp.einsum("lgn,gjpn->lgjp", c_wide, carry_state) * jnp.exp(running)[..., None]
    to_end = jnp.exp(running[-1] - running)
    carry_state = carry_state * jnp.exp(running[-1])[..., None, None] + jnp.einsum(
        "sgn,sgjp->gjpn", b_wide, scaled_x * to_end[..., None]
    )
    return (carry_state, inside + before)


def combine_states(earlier, later):
    early_state, early_log = earlier
    late_state, late_log = later
    return (early_state * jnp.exp(late_log)[..., None, None] + late_state, early_log + late_log)


def local(
    blender_incoming_features,
    entry_latent_matrix,
    exit_latent_matrix,
    unactivated_valve,
    presoftplus_strides,
    extra_attenuation,
    incoming_feature_kernel,
    entry_latent_kernel,
    exit_latent_kernel,
    stride_offset_vector,
    attenuation_speed_exponent,
    bypass_coef_vector,
    cluster_rescale_coefs,
    blender_result_matrix,
    latter_microbatch_activations,
    specialist_rescale_coefs,
    specialist_valve_matrix,
    specialist_expand_matrix,
    specialist_contract_matrix,
    specialist_picks,
    selected_specialist_coefs,
):
    tap_count = incoming_feature_kernel.shape[0]
    tok_rows = blender_incoming_features.shape[0]
    groups_local = entry_latent_matrix.shape[1] // STATE
    members_within_cluster = HEADS // SHARING_CLUSTERS
    tail_start = tok_rows - tap_count + 1
    rim_x, rim_b, rim_c = from_behind(
        (
            blender_incoming_features[tail_start:],
            entry_latent_matrix[tail_start:],
            exit_latent_matrix[tail_start:],
        ),
        EP,
        1,
    )
    conv_x_out = conv_silu(blender_incoming_features, rim_x, incoming_feature_kernel).reshape(
        tok_rows, groups_local, members_within_cluster, HEAD_DIM
    )
    conv_b_out = (
        conv_silu(entry_latent_matrix, rim_b, entry_latent_kernel)
        .astype(jnp.bfloat16)
        .reshape(tok_rows, groups_local, STATE)
    )
    conv_c_out = (
        conv_silu(exit_latent_matrix, rim_c, exit_latent_kernel)
        .astype(jnp.bfloat16)
        .reshape(tok_rows, groups_local, STATE)
    )
    stride_amount = jax.nn.softplus(presoftplus_strides + stride_offset_vector[None, :])
    attenuation_exponent = (
        -jnp.exp(attenuation_speed_exponent)[None, :] * stride_amount + extra_attenuation
    ).reshape(tok_rows, groups_local, members_within_cluster)
    scaled_x = (
        conv_x_out
        * stride_amount.reshape(tok_rows, groups_local, members_within_cluster)[..., None]
    )
    blocks = tok_rows // BLOCK

    def as_blocks(array_value):
        return array_value.reshape((blocks, BLOCK) + array_value.shape[1:])

    start_state = jnp.zeros((groups_local, members_within_cluster, HEAD_DIM, STATE), jnp.float32)
    end_state, block_out = lax.scan(
        block_step,
        start_state,
        (
            as_blocks(scaled_x),
            as_blocks(conv_b_out),
            as_blocks(conv_c_out),
            as_blocks(attenuation_exponent),
        ),
    )
    running = jnp.cumsum(attenuation_exponent, axis=0)
    enter_state = carried_in(
        (end_state, running[-1]),
        EP,
        combine_states,
        (jnp.zeros_like(end_state), jnp.zeros_like(running[-1])),
    )[0]
    carried = (
        jnp.einsum("lgn,gjpn->lgjp", conv_c_out.astype(jnp.float32), enter_state)
        * jnp.exp(running)[..., None]
    )
    ssd_out = (
        block_out.reshape(tok_rows, groups_local, members_within_cluster, HEAD_DIM)
        + carried
        + bypass_coef_vector.reshape(groups_local, members_within_cluster)[None, :, :, None]
        * conv_x_out
    )
    gated_out = ssd_out.reshape(tok_rows, -1) * jax.nn.silu(unactivated_valve.astype(jnp.float32))
    grouped = gated_out.reshape(tok_rows, groups_local, -1)
    grouped = grouped * lax.rsqrt(jnp.mean(grouped * grouped, axis=-1, keepdims=True) + NORM_EPS)
    normed = (grouped.reshape(tok_rows, -1) * cluster_rescale_coefs.astype(jnp.float32)).astype(
        jnp.bfloat16
    )
    mixed_a = summed_on_arrival(
        jnp.dot(normed, blender_result_matrix, preferred_element_type=jnp.float32).astype(
            jnp.bfloat16
        ),
        TP,
        0,
    ).astype(jnp.bfloat16)
    ep_count = lax.axis_size(EP)
    token_count = latter_microbatch_activations.shape[0]
    model_width = latter_microbatch_activations.shape[1]
    local_experts = specialist_valve_matrix.shape[0]
    expert_count = ep_count * local_experts
    capacity = 3 * token_count * TOPK // (2 * expert_count)
    slot_total = expert_count * capacity
    widened = latter_microbatch_activations.astype(jnp.float32)
    normed_b = (
        widened
        * lax.rsqrt(jnp.mean(widened * widened, axis=-1, keepdims=True) + NORM_EPS)
        * specialist_rescale_coefs.astype(jnp.float32)
    ).astype(jnp.bfloat16)
    flat_routes = specialist_picks.reshape(-1)
    assigned = flat_routes.shape[0]
    positions = jnp.arange(assigned, dtype=jnp.int32)
    earlier_same = (flat_routes[:, None] == flat_routes[None, :]) & (
        positions[None, :] < positions[:, None]
    )
    slot_rank = jnp.sum(earlier_same.astype(jnp.int32), axis=1)
    slot_of = flat_routes * capacity + slot_rank
    slot_ids = jnp.arange(slot_total, dtype=jnp.int32)
    placing = (slot_ids[:, None] == slot_of[None, :]).astype(jnp.bfloat16)
    placing = jnp.sum(placing.reshape(slot_total, token_count, TOPK), axis=2)
    outgoing = jnp.dot(placing, normed_b, preferred_element_type=jnp.float32).astype(jnp.bfloat16)
    outgoing = outgoing.reshape(ep_count, local_experts, capacity, model_width)
    slice_width = model_width // lax.axis_size(TP)
    my_columns = lax.dynamic_slice_in_dim(
        outgoing, lax.axis_index(TP) * slice_width, slice_width, 3
    )
    arrived = lax.all_to_all(my_columns, EP, split_axis=0, concat_axis=0, tiled=True)
    gathered_piece = lax.all_gather(arrived, TP, axis=3, tiled=True)
    gate_sum = jnp.einsum(
        "sejd,edf->sejf",
        gathered_piece,
        specialist_valve_matrix,
        preferred_element_type=jnp.float32,
    )
    up_sum = jnp.einsum(
        "sejd,edf->sejf",
        gathered_piece,
        specialist_expand_matrix,
        preferred_element_type=jnp.float32,
    )
    hidden = (jax.nn.silu(gate_sum) * up_sum).astype(jnp.bfloat16)
    partial_out = jnp.einsum(
        "sejf,efd->sejd", hidden, specialist_contract_matrix, preferred_element_type=jnp.float32
    )
    summed = (
        summed_rows(partial_out.astype(jnp.bfloat16), TP, 3)
        .astype(jnp.float32)
        .astype(jnp.bfloat16)
    )
    returned = lax.all_to_all(summed, EP, split_axis=0, concat_axis=0, tiled=True)
    returned = returned.reshape(slot_total, -1)
    token_slots = slot_of.reshape(token_count, TOPK)
    combined = jnp.zeros((token_count, returned.shape[1]), jnp.float32)
    for pick_index in range(TOPK):
        selecting = (token_slots[:, pick_index][:, None] == slot_ids[None, :]).astype(jnp.bfloat16)
        chosen_rows = jnp.dot(selecting, returned, preferred_element_type=jnp.float32)
        combined = combined + chosen_rows * selected_specialist_coefs[:, pick_index][:, None]
    mixed_b = combined.astype(jnp.bfloat16)
    return (mixed_a, mixed_b)


def solution(mesh):
    split = Mesh(mesh.devices.reshape(8, 4, 8, 2), ("ep_0", "ep_1", "tp_0", "tp_1"))
    in_specs = (
        P(EP, TP),
        P(EP, TP),
        P(EP, TP),
        P(EP, TP),
        P(EP, TP),
        P(EP, TP),
        P(None, TP),
        P(None, TP),
        P(None, TP),
        P(TP),
        P(TP),
        P(TP),
        P(TP),
        P(TP, None),
        P(EP, None),
        P(),
        P(EP, None, TP),
        P(EP, None, TP),
        P(EP, TP, None),
        P(EP, None),
        P(EP, None),
    )
    out_specs = (P(EP_TP, None), P(EP, TP))
    return jax.shard_map(local, mesh=split, in_specs=in_specs, out_specs=out_specs, check_vma=False)
```

profile of v0, /device:TPU:8, one launch (start us, length us, event | category | flops | bytes accessed | tf_op | source)
XLA Modules:
  0.0 217.6 jit_solution(4881775239269224496)
XLA Ops:
  12.1 2.5 %convolution_convert_fusion.1 = bf16[768,2048]{1,0:T(8,128)(2,1)S(1)} fusion(bf16[768,256]{1,0:T(8,128)(2,1)S(1)} %fusion.71, bf16[256,2048]{1,0:T(8,128)(2,1)} %param.37, f32[2048]{0:T(1024)S(1)} %convert_element_type.381, f32[256]{0:T(256)S(1)} %add_rsqrt_fusion), kind=kOutput, calls=%fused_computation.46 | convolution fusion | flops 808976384 | bytes 4596736 | tf_op jit(solution)/shard_map/dot_general | solution.py:235
  14.7 24.7 %all_to_all.15 = bf16[32,1,24,128]{3,2,1,0:T(8,128)(2,1)} all-to-all(bf16[32,1,24,128]{3,2,1,0:T(8,128)(2,1)S(1)} %constant_dynamic-slice_fusion.2), channel_id=1, replica_groups=mesh['ep_0'=8,'ep_1'=4,'tp_0'=8,'tp_1'=2] {'ep_0','ep_1'}, dimensions={0} | all-to-all | bytes 393216 | tf_op jit(solution)/shard_map/all_to_all | solution.py:241
  41.4 3.4 %collective-permute-start.2 = (bf16[3,128]{1,0:T(4,128)(2,1)S(1)}, bf16[3,128]{1,0:T(4,128)(2,1)S(1)}, u32[]{:S(2)}, u32[]{:S(2)}) collective-permute-start(bf16[3,128]{1,0:T(4,128)(2,1)S(1)} %slice.198), channel_id=1, source_target_pairs={{0,16},{16,32},{32,48},{48,64},{64,80},{80,96},{96,112},{112,128},... | collective-permute-start | bytes 2312 | tf_op jit(solution)/shard_map/ppermute | solution.py:22
  46.8 3.3 %collective-permute-start.1 = (bf16[3,128]{1,0:T(4,128)(2,1)S(1)}, bf16[3,128]{1,0:T(4,128)(2,1)S(1)}, u32[]{:S(2)}, u32[]{:S(2)}) collective-permute-start(bf16[3,128]{1,0:T(4,128)(2,1)S(1)} %slice.189), channel_id=1, source_target_pairs={{0,16},{16,32},{32,48},{48,64},{64,80},{80,96},{96,112},{112,128},... | collective-permute-start | bytes 2312 | tf_op jit(solution)/shard_map/ppermute | solution.py:22
  50.0 9.3 %all_gather.21 = bf16[4,1,4]{2,1,0:T(2,128)(2,1)S(1)} all-gather(bf16[1,1,4]{2,1,0:T(2,128)(2,1)S(1)} %slice.260), channel_id=1, replica_groups=mesh['ep_0'=8,'ep_1'=4,'tp_0'=8,'tp_1'=2] {'ep_1'}, dimensions={0}, use_global_device_ids=true | all-gather | bytes 40 | tf_op jit(solution)/shard_map/all_gather | solution.py:37
  59.4 13.9 %all_gather.22 = bf16[8,1,4]{2,1,0:T(2,128)(2,1)S(1)} all-gather(bf16[1,1,4]{2,1,0:T(2,128)(2,1)S(1)} %get-tuple-element.133), channel_id=1, replica_groups=mesh['ep_0'=8,'ep_1'=4,'tp_0'=8,'tp_1'=2] {'ep_0'}, dimensions={0}, use_global_device_ids=true | all-gather | bytes 72 | tf_op jit(solution)/shard_map/all_gather | solution.py:37
  74.9 6.9 %all-gather.3.cloned.1.call-done = bf16[32,1,24,2048]{3,2,0,1:T(8,128)(2,1)} async-done(((bf16[32,1,24,128]{3,2,0,1:T(8,128)(2,1)}), bf16[32,1,24,2048]{3,2,0,1:T(8,128)(2,1)}) %all-gather.3.cloned.1.call-update) | async-done | bytes 3145744 | tf_op jit(solution)/shard_map/all_gather | solution.py:242
  81.8 4.1 %fusion.44 = f32[32,1,24,256]{3,2,0,1:T(8,128)} fusion(bf16[32,1,24,2048]{3,2,0,1:T(8,128)(2,1)} %all-gather.3.cloned.1.call-done, bf16[1,2048,256]{2,1,0:T(8,128)(2,1)} %param.39), kind=kOutput, calls=%fused_computation.60 | convolution fusion | flops 805306368 | bytes 4980736 | tf_op jit(solution)/shard_map/sejd,edf->sejf/dot_general | solution.py:243
  85.8 7.5 %fusion.39 = bf16[32,1,24,2048]{3,2,0,1:T(8,128)(2,1)} fusion(bf16[1,256,2048]{2,1,0:T(8,128)(2,1)S(1)} %copy-done, bf16[32,1,24,2048]{3,2,0,1:T(8,128)(2,1)} %all-gather.3.cloned.1.call-done, bf16[1,2048,256]{2,1,0:T(8,128)(2,1)} %param.40, f32[32,1,24,256]{3,2,0,1:T(8,128)} %fusion.44), kind=kOutput, calls=%fused_computation.51 | convolution fusion | flops 1613365248 | bytes 9175040 | tf_op jit(solution)/shard_map/sejf,efd->sejd/dot_general | solution.py:256
  94.3 16.0 %while.13 = (s32[]{:T(128)}, f32[1,4,64,128]{3,2,1,0:T(8,128)S(1)}, f32[4,64,1,4,64]{1,0,4,3,2:T(4,128)S(1)}, f32[4,64,1,4]{3,1,2,0:T(8,128)S(1)}, f32[4,64,1,4,...) while((s32[]{:T(128)}, f32[1,4,64,128]{3,2,1,0:T(8,128)S(1)}, ...), condition=%wide.region_2.3_spmd.clone, body=%wide.region_0.2_spmd.clone.sunk | while | flops 11800579 | bytes 1400524 | solution.py:171
  95.3 2.8 %dynamic_update_slice.6 = f32[4,64,1,4,64]{1,0,4,3,2:T(4,128)S(1)} dynamic-update-slice(f32[4,64,1,4,64]{1,0,4,3,2:T(4,128)S(1)} %get-tuple-element.209, f32[1,64,1,4,64]{1,0,4,3,2:T(1,128)S(1)} %bitcast.305, s32[]{:T(128)} %get-tuple-element.207, s32[]{:T(128)} %constant.33.clone.1..sunk, s32[]{:T(128)} %constant.33.clone.1..sunk, s32[]{:T(128)} %constant.33.clone.1..sunk, s32[]{:T(128)} %constant.33.clone.1..sunk) | dynamic-update-slice | bytes 131076 | tf_op jit(solution)/shard_map/while/body/jit(dynamic_update_index_in_dim)/dynamic_update_slice | solution.py:171
  99.3 2.8 %dynamic_update_slice.6 = f32[4,64,1,4,64]{1,0,4,3,2:T(4,128)S(1)} dynamic-update-slice(f32[4,64,1,4,64]{1,0,4,3,2:T(4,128)S(1)} %get-tuple-element.209, f32[1,64,1,4,64]{1,0,4,3,2:T(1,128)S(1)} %bitcast.305, s32[]{:T(128)} %get-tuple-element.207, s32[]{:T(128)} %constant.33.clone.1..sunk, s32[]{:T(128)} %constant.33.clone.1..sunk, s32[]{:T(128)} %constant.33.clone.1..sunk, s32[]{:T(128)} %constant.33.clone.1..sunk) | dynamic-update-slice | bytes 131076 | tf_op jit(solution)/shard_map/while/body/jit(dynamic_update_index_in_dim)/dynamic_update_slice | solution.py:171
  103.3 2.8 %dynamic_update_slice.6 = f32[4,64,1,4,64]{1,0,4,3,2:T(4,128)S(1)} dynamic-update-slice(f32[4,64,1,4,64]{1,0,4,3,2:T(4,128)S(1)} %get-tuple-element.209, f32[1,64,1,4,64]{1,0,4,3,2:T(1,128)S(1)} %bitcast.305, s32[]{:T(128)} %get-tuple-element.207, s32[]{:T(128)} %constant.33.clone.1..sunk, s32[]{:T(128)} %constant.33.clone.1..sunk, s32[]{:T(128)} %constant.33.clone.1..sunk, s32[]{:T(128)} %constant.33.clone.1..sunk) | dynamic-update-slice | bytes 131076 | tf_op jit(solution)/shard_map/while/body/jit(dynamic_update_index_in_dim)/dynamic_update_slice | solution.py:171
  107.3 2.8 %dynamic_update_slice.6 = f32[4,64,1,4,64]{1,0,4,3,2:T(4,128)S(1)} dynamic-update-slice(f32[4,64,1,4,64]{1,0,4,3,2:T(4,128)S(1)} %get-tuple-element.209, f32[1,64,1,4,64]{1,0,4,3,2:T(1,128)S(1)} %bitcast.305, s32[]{:T(128)} %get-tuple-element.207, s32[]{:T(128)} %constant.33.clone.1..sunk, s32[]{:T(128)} %constant.33.clone.1..sunk, s32[]{:T(128)} %constant.33.clone.1..sunk, s32[]{:T(128)} %constant.33.clone.1..sunk) | dynamic-update-slice | bytes 131076 | tf_op jit(solution)/shard_map/while/body/jit(dynamic_update_index_in_dim)/dynamic_update_slice | solution.py:171
  110.8 12.6 %all-gather = bf16[4,4,64,128]{3,2,1,0:T(8,128)(2,1)S(1)} all-gather(bf16[1,4,64,128]{3,2,1,0:T(8,128)(2,1)S(1)} %convert_element_type.353), channel_id=2, replica_groups=mesh['ep_0'=8,'ep_1'=4,'tp_0'=8,'tp_1'=2] {'ep_1'}, dimensions={0}, use_global_device_ids=true | all-gather | bytes 327680 | tf_op jit(solution)/shard_map/all_gather | solution.py:37
  123.6 27.3 %all_gather.25 = bf16[8,1,4,64,128]{4,3,2,1,0:T(8,128)(2,1)S(1)} all-gather(bf16[1,1,4,64,128]{4,3,2,1,0:T(8,128)(2,1)S(1)} %fusion.134), channel_id=1, replica_groups=mesh['ep_0'=8,'ep_1'=4,'tp_0'=8,'tp_1'=2] {'ep_0'}, dimensions={0}, use_global_device_ids=true | all-gather | bytes 589824 | tf_op jit(solution)/shard_map/all_gather | solution.py:37
  151.6 2.7 %convolution_convert_fusion.2 = bf16[256,2048]{1,0:T(8,128)(2,1)} fusion(bf16[256,2048]{1,0:T(8,128)(2,1)} %param.36, f32[256]{0:T(256)S(1)} %convert_element_type.375, f32[256]{0:T(256)S(1)} %add_rsqrt_fusion.1, f32[256,256]{1,0:T(8,128)S(1)} %copy.134, bf16[256,256]{1,0:T(8,128)(2,1)S(1)} %copy-done.3), kind=kOutput, calls=%fused_computation.54 | convolution fusion | flops 269549568 | bytes 2492416 | tf_op jit(solution)/shard_map/dot_general | solution.py:205
  154.3 5.4 %all-to-all-start = ((bf16[16,16,2048]{2,1,0:T(8,128)(2,1)}), bf16[16,16,2048]{2,1,0:T(8,128)(2,1)}, u32[]{:S(2)}, u32[]{:S(2)}) async-start(bf16[16,16,2048]{2,1,0:T(8,128)(2,1)} %bitcast.49), calls=%async_computation | async-start | bytes 2097152 | tf_op jit(solution)/shard_map/all_to_all | solution.py:59
  159.9 3.8 %copy.143 = bf16[32,1,24,256]{2,0,1,3:T(8,128)(2,1)S(1)} copy(bf16[32,1,24,256]{3,2,0,1:T(8,128)(2,1)} %reduce-scatter.5.cloned.1.call-done) | data formatting | bytes 786432
  163.7 4.2 %reshape.641 = bf16[256,768]{1,0:T(8,128)(2,1)} reshape(bf16[256,1,32,24]{3,2,1,0:T(8,128)(2,1)S(1)} %bitcast.307) | data formatting | bytes 786432
  168.0 15.1 %reduce-scatter.7.cloned.1.call-done = bf16[128,768]{1,0:T(8,128)(2,1)} async-done(((bf16[256,768]{1,0:T(8,128)(2,1)}), bf16[128,768]{1,0:T(8,128)(2,1)}) %reduce-scatter.7.cloned.1.call-update) | async-done | bytes 196624
  183.1 2.6 %reshape.642 = bf16[128,1,32,24]{3,2,1,0:T(8,128)(2,1)S(1)} reshape(bf16[128,768]{1,0:T(8,128)(2,1)} %reduce-scatter.7.cloned.1.call-done) | data formatting | bytes 393216
  187.5 10.2 %all-to-all-start.2 = ((bf16[32,1,24,128]{3,2,1,0:T(8,128)(2,1)}), bf16[32,1,24,128]{3,2,1,0:T(8,128)(2,1)S(1)}, u32[]{:S(2)}, u32[]{:S(2)}) async-start(bf16[32,1,24,128]{3,2,1,0:T(8,128)(2,1)} %bitcast.73), calls=%async_computation.3 | async-start | bytes 393216 | tf_op jit(solution)/shard_map/all_to_all | solution.py:264
  199.7 10.1 %all-to-all-done.2 = bf16[32,1,24,128]{3,2,1,0:T(8,128)(2,1)S(1)} async-done(((bf16[32,1,24,128]{3,2,1,0:T(8,128)(2,1)}), bf16[32,1,24,128]{3,2,1,0:T(8,128)(2,1)S(1)}, u32[]{:S(2)}, u32[]{:S(2)}) %all-to-all-start.2) | async-done | bytes 196640 | tf_op jit(solution)/shard_map/all_to_all | solution.py:264
  (161 shorter events, 22.3 us)
Async XLA Ops:
  7.2 78.7 %copy-start = (bf16[1,256,2048]{2,1,0:T(8,128)(2,1)S(1)}, bf16[1,256,2048]{2,1,0:T(8,128)(2,1)}, u32[]{:S(2)}) copy-start(bf16[1,256,2048]{2,1,0:T(8,128)(2,1)} %param.41) | copy-start | bytes 3145732
  7.2 74.6 %all-gather.3.cloned.1.call-start = ((), (), s32[]{:S(2)}) async-start(), calls=%async_computation.5 | async-start | bytes 3342336 | tf_op jit(solution)/shard_map/all_gather | solution.py:242
  12.0 27.5 %copy-start.2 = (bf16[256,256]{1,0:T(8,128)(2,1)S(1)}, bf16[256,256]{1,0:T(8,128)(2,1)}, u32[]{:S(2)}) copy-start(bf16[256,256]{1,0:T(8,128)(2,1)} %param.23) | copy-start | bytes 393220
  12.0 29.3 %copy-start.4 = (bf16[256,128]{1,0:T(8,128)(2,1)S(1)}, bf16[256,128]{1,0:T(8,128)(2,1)}, u32[]{:S(2)}) copy-start(bf16[256,128]{1,0:T(8,128)(2,1)} %param.25) | copy-start | bytes 196612
  12.0 32.7 %copy-start.13 = (f32[4]{0:T(128)S(1)}, f32[4]{0:T(128)}, u32[]{:S(2)}) copy-start(f32[4]{0:T(128)} %param.33) | copy-start | bytes 52
  12.0 32.7 %copy-start.7 = (f32[256,4]{0,1:T(4,128)S(1)}, f32[256,4]{0,1:T(4,128)}, u32[]{:S(2)}) copy-start(f32[256,4]{0,1:T(4,128)} %param.28) | copy-start | bytes 12292
  12.0 32.7 %copy-start.8 = (f32[256,4]{0,1:T(4,128)S(1)}, f32[256,4]{0,1:T(4,128)}, u32[]{:S(2)}) copy-start(f32[256,4]{0,1:T(4,128)} %param.27) | copy-start | bytes 12292
  12.1 32.7 %copy-start.12 = (f32[4]{0:T(128)S(1)}, f32[4]{0:T(128)}, u32[]{:S(2)}) copy-start(f32[4]{0:T(128)} %param.32) | copy-start | bytes 52
  12.1 34.3 %copy-start.5 = (bf16[256,128]{1,0:T(8,128)(2,1)S(1)}, bf16[256,128]{1,0:T(8,128)(2,1)}, u32[]{:S(2)}) copy-start(bf16[256,128]{1,0:T(8,128)(2,1)} %param.24) | copy-start | bytes 196612
  12.1 61.4 %copy-start.10 = (bf16[4,128]{1,0:T(4,128)(2,1)S(1)}, bf16[4,128]{1,0:T(4,128)(2,1)}, u32[]{:S(2)}) copy-start(bf16[4,128]{1,0:T(4,128)(2,1)} %param.31) | copy-start | bytes 3076
  12.1 61.4 %copy-start.11 = (bf16[4,128]{1,0:T(4,128)(2,1)S(1)}, bf16[4,128]{1,0:T(4,128)(2,1)}, u32[]{:S(2)}) copy-start(bf16[4,128]{1,0:T(4,128)(2,1)} %param.30) | copy-start | bytes 3076
  12.1 61.4 %copy-start.6 = (bf16[4,256]{1,0:T(4,128)(2,1)S(1)}, bf16[4,256]{1,0:T(4,128)(2,1)}, u32[]{:S(2)}) copy-start(bf16[4,256]{1,0:T(4,128)(2,1)} %param.29) | copy-start | bytes 6148
  12.1 61.7 %copy-start.14 = (bf16[256]{0:T(256)(128)(2,1)S(1)}, bf16[256]{0:T(256)(128)(2,1)}, u32[]{:S(2)}) copy-start(bf16[256]{0:T(256)(128)(2,1)} %param.35) | copy-start | bytes 1540
  39.4 120.5 %reduce-scatter.5.cloned.1.call-start = ((), (), s32[]{:S(2)}) async-start(), calls=%async_computation.6 | async-start | bytes 3538944 | tf_op jit(solution)/shard_map/reduce_scatter | solution.py:65
  39.5 34.6 %collective-permute-start = (bf16[3,256]{1,0:T(4,128)(2,1)S(1)}, bf16[3,256]{1,0:T(4,128)(2,1)S(1)}, u32[]{:S(2)}, u32[]{:S(2)}) collective-permute-start(bf16[3,256]{1,0:T(4,128)(2,1)S(1)} %slice.180), channel_id=1, source_target_pairs={{0,16},{16,32},{32,48},{48,64},{64,80},{80,96},{96,112},{112,128},... | collective-permute-start | bytes 4616 | tf_op jit(solution)/shard_map/ppermute | solution.py:22
  41.4 32.4 %collective-permute-start.2 = (bf16[3,128]{1,0:T(4,128)(2,1)S(1)}, bf16[3,128]{1,0:T(4,128)(2,1)S(1)}, u32[]{:S(2)}, u32[]{:S(2)}) collective-permute-start(bf16[3,128]{1,0:T(4,128)(2,1)S(1)} %slice.198), channel_id=1, source_target_pairs={{0,16},{16,32},{32,48},{48,64},{64,80},{80,96},{96,112},{112,128},... | collective-permute-start | bytes 2312 | tf_op jit(solution)/shard_map/ppermute | solution.py:22
  46.8 27.1 %collective-permute-start.1 = (bf16[3,128]{1,0:T(4,128)(2,1)S(1)}, bf16[3,128]{1,0:T(4,128)(2,1)S(1)}, u32[]{:S(2)}, u32[]{:S(2)}) collective-permute-start(bf16[3,128]{1,0:T(4,128)(2,1)S(1)} %slice.189), channel_id=1, source_target_pairs={{0,16},{16,32},{32,48},{48,64},{64,80},{80,96},{96,112},{112,128},... | collective-permute-start | bytes 2312 | tf_op jit(solution)/shard_map/ppermute | solution.py:22
  93.3 1.0 copy-start.1
  94.3 56.5 %copy-start.15 = (f32[4]{0:T(128)S(1)}, f32[4]{0:T(128)}, u32[]{:S(2)}) copy-start(f32[4]{0:T(128)} %param.34) | copy-start | bytes 52
  110.3 41.1 %copy-start.3 = (bf16[256,256]{1,0:T(8,128)(2,1)S(1)}, bf16[256,256]{1,0:T(8,128)(2,1)}, u32[]{:S(2)}) copy-start(bf16[256,256]{1,0:T(8,128)(2,1)} %param.26) | copy-start | bytes 393220
  154.3 33.2 %all-to-all-start = ((bf16[16,16,2048]{2,1,0:T(8,128)(2,1)}), bf16[16,16,2048]{2,1,0:T(8,128)(2,1)}, u32[]{:S(2)}, u32[]{:S(2)}) async-start(bf16[16,16,2048]{2,1,0:T(8,128)(2,1)} %bitcast.49), calls=%async_computation | async-start | bytes 2097152 | tf_op jit(solution)/shard_map/all_to_all | solution.py:59
  159.7 23.4 %reduce-scatter.7.cloned.1.call-start = ((), (), s32[]{:S(2)}) async-start(), calls=%async_computation.7 | async-start | bytes 589824
  163.7 34.0 %copy-start.9 = (f32[256,2]{0,1:T(2,128)S(1)}, f32[256,2]{0,1:T(2,128)}, u32[]{:S(2)}) copy-start(f32[256,2]{0,1:T(2,128)} %param.43) | copy-start | bytes 6148
  187.5 22.3 %all-to-all-start.2 = ((bf16[32,1,24,128]{3,2,1,0:T(8,128)(2,1)}), bf16[32,1,24,128]{3,2,1,0:T(8,128)(2,1)S(1)}, u32[]{:S(2)}, u32[]{:S(2)}) async-start(bf16[32,1,24,128]{3,2,1,0:T(8,128)(2,1)} %bitcast.73), calls=%async_computation.3 | async-start | bytes 393216 | tf_op jit(solution)/shard_map/all_to_all | solution.py:264
Sparse Core Ops, SparseCore 0:
  39.5 42.2 all-gather.2
  93.4 48.1 reduce-scatter.4
  168.1 14.9 reduce-scatter.6
where the time goes:
time: 218 us
  blocking collectives  87.9 us (40%)
  waiting for transfers between devices  32.2 us (15%)
  local copies, waits for them, and re-layouts  28.7 us (13%)
  starting transfers between devices  24.4 us (11%)
  matrix products  21 us (10%)
  between operations  14.4 us (7%)
  other arithmetic  8.82 us (4%)
    all_gather x4, blocking collectives, carried_in(): lax.all_gather(part.astype(kind), axis)  63.2 us
    all_to_all x1, blocking collectives, local(): lax.all_to_all(my_columns, EP, split_axis=0, concat_axis=0, tiled=True)  24.7 us
    unnamed x4, waiting for transfers between devices  15.2 us
    unnamed x37, local copies, waits for them, and re-layouts  14.4 us
    dynamic_update_slice x4, local copies, waits for them, and re-layouts, local(): lax.scan(block_step, start_state, (as_blocks(scaled_x), as_blocks(conv_b_...  11.2 us
    all_to_all x1, starting transfers between devices, local(): lax.all_to_all(summed, EP, split_axis=0, concat_axis=0, tiled=True)  10.2 us
    all_to_all x1, waiting for transfers between devices, local(): lax.all_to_all(summed, EP, split_axis=0, concat_axis=0, tiled=True)  10.1 us
    ppermute x3, starting transfers between devices, from_behind(): return lax.ppermute(block, axis, route)  8.48 us
  transfers between devices with their start and end apart: 8, of which 3 were waited for; matrix products, arithmetic and copies ran while one was open for 17% of the time, Pallas kernels for 0%

commit v1 on v0

--- a/solution.py
+++ b/solution.py
@@ -239,7 +239,9 @@
         outgoing, lax.axis_index(TP) * slice_width, slice_width, 3
     )
     arrived = lax.all_to_all(my_columns, EP, split_axis=0, concat_axis=0, tiled=True)
-    gathered_piece = lax.all_gather(arrived, TP, axis=3, tiled=True)
+    gathered_piece = jnp.concatenate(
+        lax.all_to_all(jnp.stack([arrived] * lax.axis_size(TP)), TP, 0, 0), axis=3
+    )
     gate_sum = jnp.einsum(
         "sejd,edf->sejf",
         gathered_piece,

time: 218 us -> 262 us (1.20)
  waiting for transfers between devices: 32.2 us -> 56.5 us
  local copies, waits for them, and re-layouts: 28.7 us -> 44.1 us
  starting transfers between devices: 24.4 us -> 32.9 us
    all_to_all x0 -> x1, waiting for transfers between devices: none -> 34.1 us  [local(): lax.all_to_all(jnp.stack([arrived] * lax.axis_size(TP)), TP, 0, 0)]
    another operation x3 -> x5, local copies, waits for them, and re-layouts: 0.15 us -> 8.23 us
    all_to_all x0 -> x1, starting transfers between devices: none -> 7.71 us  [local(): lax.all_to_all(jnp.stack([arrived] * lax.axis_size(TP)), TP, 0, 0)]
    reshape x1 -> x2, local copies, waits for them, and re-layouts: 0.01 us -> 7.21 us  [the longest x1 7.2 us: local(): jnp.concatenate(lax.all_to_all(jnp.stack([arrived] * lax.axis_size(TP)),...]
    all_gather x1 -> x0, waiting for transfers between devices: 6.89 us -> none  [local(): gathered_piece = lax.all_gather(arrived, TP, axis=3, tiled=True)]
    unnamed x4 -> x3, waiting for transfers between devices: 15.2 us -> 11.6 us
    unnamed x37 -> x39, local copies, waits for them, and re-layouts: 14.4 us -> 14.4 us
  transfers between devices with their start and end apart: 8 -> 8, of which waited for: 3 -> 4; matrix products, arithmetic and copies ran while one was open for 17% -> 14% of each run, Pallas kernels for 0% -> 0%
where the time goes in v1:
time: 262 us; the launch traced here: 261 us
  blocking collectives  85.7 us (33%)
  waiting for transfers between devices  56.5 us (22%)
  local copies, waits for them, and re-layouts  44.1 us (17%)
  starting transfers between devices  32.9 us (13%)
  matrix products  18.5 us (7%)
  between operations  14.7 us (6%)
  other arithmetic  8.82 us (3%)
    all_gather x4, blocking collectives, carried_in(): lax.all_gather(part.astype(kind), axis)  61.1 us
    all_to_all x1, waiting for transfers between devices, local(): lax.all_to_all(jnp.stack([arrived] * lax.axis_size(TP)), TP, 0, 0)  34.1 us
    all_to_all x1, blocking collectives, local(): lax.all_to_all(my_columns, EP, split_axis=0, concat_axis=0, tiled=True)  24.6 us
    unnamed x39, local copies, waits for them, and re-layouts  14.4 us
    unnamed x3, waiting for transfers between devices  11.6 us
    dynamic_update_slice x4, local copies, waits for them, and re-layouts, local(): lax.scan(block_step, start_state, (as_blocks(scaled_x), as_blocks(conv_b_...  11.2 us
    all_to_all x1, waiting for transfers between devices, local(): lax.all_to_all(summed, EP, split_axis=0, concat_axis=0, tiled=True)  10.1 us
    all_to_all x1, starting transfers between devices, local(): lax.all_to_all(summed, EP, split_axis=0, concat_axis=0, tiled=True)  9.58 us
  transfers between devices with their start and end apart: 8, of which 4 were waited for; matrix products, arithmetic and copies ran while one was open for 14% of the time, Pallas kernels for 0%

profile of v1, /device:TPU:8, one launch (start us, length us, event | category | flops | bytes accessed | tf_op | source)
XLA Modules:
  0.0 261.4 jit_solution(4554807395674338553)
XLA Ops:
  14.4 24.6 %all_to_all.23 = bf16[32,1,24,128]{3,2,1,0:T(8,128)(2,1)S(1)} all-to-all(bf16[32,1,24,128]{3,2,1,0:T(8,128)(2,1)S(1)} %constant_dynamic-slice_fusion.2), channel_id=1, replica_groups=mesh['ep_0'=8,'ep_1'=4,'tp_0'=8,'tp_1'=2] {'ep_0','ep_1'}, dimensions={0} | all-to-all | bytes 393216 | tf_op jit(solution)/shard_map/all_to_all | solution.py:241
  41.4 7.7 %all-to-all-start.2 = ((bf16[16,32,1,24,128]{4,3,1,2,0:T(8,128)(2,1)}), bf16[16,32,1,24,128]{4,3,1,2,0:T(8,128)(2,1)}, u32[]{:S(2)}, u32[]{:S(2)}) async-start(bf16[16,32,1,24,128]{4,3,1,2,0:T(8,128)(2,1)} %stack.2), calls=%async_computation.2 | async-start | bytes 6291456 | tf_op jit(solution)/shard_map/all_to_all | solution.py:243
  51.0 3.4 %collective-permute-start.2 = (bf16[3,128]{1,0:T(4,128)(2,1)S(1)}, bf16[3,128]{1,0:T(4,128)(2,1)S(1)}, u32[]{:S(2)}, u32[]{:S(2)}) collective-permute-start(bf16[3,128]{1,0:T(4,128)(2,1)S(1)} %slice.198), channel_id=1, source_target_pairs={{0,16},{16,32},{32,48},{48,64},{64,80},{80,96},{96,112},{112,128},... | collective-permute-start | bytes 2312 | tf_op jit(solution)/shard_map/ppermute | solution.py:22
  56.4 3.3 %collective-permute-start.1 = (bf16[3,128]{1,0:T(4,128)(2,1)S(1)}, bf16[3,128]{1,0:T(4,128)(2,1)S(1)}, u32[]{:S(2)}, u32[]{:S(2)}) collective-permute-start(bf16[3,128]{1,0:T(4,128)(2,1)S(1)} %slice.189), channel_id=1, source_target_pairs={{0,16},{16,32},{32,48},{48,64},{64,80},{80,96},{96,112},{112,128},... | collective-permute-start | bytes 2312 | tf_op jit(solution)/shard_map/ppermute | solution.py:22
  59.7 9.3 %all_gather.18 = bf16[4,1,4]{2,1,0:T(2,128)(2,1)S(1)} all-gather(bf16[1,1,4]{2,1,0:T(2,128)(2,1)S(1)} %slice.260), channel_id=1, replica_groups=mesh['ep_0'=8,'ep_1'=4,'tp_0'=8,'tp_1'=2] {'ep_1'}, dimensions={0}, use_global_device_ids=true | all-gather | bytes 40 | tf_op jit(solution)/shard_map/all_gather | solution.py:37
  69.0 14.1 %all_gather.19 = bf16[8,1,4]{2,1,0:T(2,128)(2,1)S(1)} all-gather(bf16[1,1,4]{2,1,0:T(2,128)(2,1)S(1)} %get-tuple-element.133), channel_id=1, replica_groups=mesh['ep_0'=8,'ep_1'=4,'tp_0'=8,'tp_1'=2] {'ep_0'}, dimensions={0}, use_global_device_ids=true | all-gather | bytes 72 | tf_op jit(solution)/shard_map/all_gather | solution.py:37
  84.7 34.1 %all-to-all-done.2 = bf16[16,32,1,24,128]{4,3,1,2,0:T(8,128)(2,1)} async-done(((bf16[16,32,1,24,128]{4,3,1,2,0:T(8,128)(2,1)}), bf16[16,32,1,24,128]{4,3,1,2,0:T(8,128)(2,1)}, u32[]{:S(2)}, u32[]{:S(2)}) %all-to-all-start.2) | async-done | bytes 3145760 | tf_op jit(solution)/shard_map/all_to_all | solution.py:243
  118.9 7.2 %copy.138 = bf16[32,1,24,16,128]{4,3,2,0,1:T(8,128)(2,1)} copy(bf16[32,1,24,16,128]{4,2,0,1,3:T(8,128)(2,1)} %bitcast.54) | data formatting | bytes 6291456 | tf_op jit(solution)/shard_map/reshape | solution.py:242
  126.1 5.8 %reshape.623 = bf16[32,24,2048]{2,1,0:T(8,128)(2,1)} reshape(bf16[32,1,24,16,128]{4,3,2,0,1:T(8,128)(2,1)} %copy.138) | data formatting | bytes 6291456 | tf_op jit(solution)/shard_map/reshape.63
  131.9 3.1 %convolution_bitcast_fusion.5 = f32[32,1,24,256]{3,2,0,1:T(8,128)S(1)} fusion(bf16[32,24,2048]{2,1,0:T(8,128)(2,1)} %reshape.623, bf16[1,2048,256]{2,1,0:T(8,128)(2,1)} %param.39), kind=kOutput, calls=%fused_computation.57 | convolution fusion | flops 805306368 | bytes 4980736 | tf_op jit(solution)/shard_map/sejd,edf->sejf/dot_general | solution.py:245
  135.0 7.2 %fusion.35 = bf16[32,1,24,2048]{3,2,0,1:T(8,128)(2,1)} fusion(bf16[1,256,2048]{2,1,0:T(8,128)(2,1)S(1)} %copy-done, bf16[32,24,2048]{2,1,0:T(8,128)(2,1)} %reshape.623, bf16[1,2048,256]{2,1,0:T(8,128)(2,1)} %param.40, f32[32,1,24,256]{3,2,0,1:T(8,128)S(1)} %convolution_bitcast_fusion.5), kind=kOutput, calls=%fused_computation.47 | convolution fusion | flops 1613365248 | bytes 9175040 | tf_op jit(solution)/shard_map/sejf,efd->sejd/dot_general | solution.py:258
  143.3 15.9 %while.13 = (s32[]{:T(128)}, f32[1,4,64,128]{3,2,1,0:T(8,128)S(1)}, f32[4,64,1,4,64]{1,0,4,3,2:T(4,128)S(1)}, f32[4,64,1,4]{3,1,2,0:T(8,128)S(1)}, f32[4,64,1,4,...) while((s32[]{:T(128)}, f32[1,4,64,128]{3,2,1,0:T(8,128)S(1)}, ...), condition=%wide.region_2.3_spmd.clone, body=%wide.region_0.2_spmd.clone.sunk | while | flops 11800579 | bytes 1400524 | solution.py:171
  144.3 2.8 %dynamic_update_slice.6 = f32[4,64,1,4,64]{1,0,4,3,2:T(4,128)S(1)} dynamic-update-slice(f32[4,64,1,4,64]{1,0,4,3,2:T(4,128)S(1)} %get-tuple-element.209, f32[1,64,1,4,64]{1,0,4,3,2:T(1,128)S(1)} %bitcast.295, s32[]{:T(128)} %get-tuple-element.207, s32[]{:T(128)} %constant.33.clone.1..sunk, s32[]{:T(128)} %constant.33.clone.1..sunk, s32[]{:T(128)} %constant.33.clone.1..sunk, s32[]{:T(128)} %constant.33.clone.1..sunk) | dynamic-update-slice | bytes 131076 | tf_op jit(solution)/shard_map/while/body/jit(dynamic_update_index_in_dim)/dynamic_update_slice | solution.py:171
  148.3 2.8 %dynamic_update_slice.6 = f32[4,64,1,4,64]{1,0,4,3,2:T(4,128)S(1)} dynamic-update-slice(f32[4,64,1,4,64]{1,0,4,3,2:T(4,128)S(1)} %get-tuple-element.209, f32[1,64,1,4,64]{1,0,4,3,2:T(1,128)S(1)} %bitcast.295, s32[]{:T(128)} %get-tuple-element.207, s32[]{:T(128)} %constant.33.clone.1..sunk, s32[]{:T(128)} %constant.33.clone.1..sunk, s32[]{:T(128)} %constant.33.clone.1..sunk, s32[]{:T(128)} %constant.33.clone.1..sunk) | dynamic-update-slice | bytes 131076 | tf_op jit(solution)/shard_map/while/body/jit(dynamic_update_index_in_dim)/dynamic_update_slice | solution.py:171
  152.3 2.8 %dynamic_update_slice.6 = f32[4,64,1,4,64]{1,0,4,3,2:T(4,128)S(1)} dynamic-update-slice(f32[4,64,1,4,64]{1,0,4,3,2:T(4,128)S(1)} %get-tuple-element.209, f32[1,64,1,4,64]{1,0,4,3,2:T(1,128)S(1)} %bitcast.295, s32[]{:T(128)} %get-tuple-element.207, s32[]{:T(128)} %constant.33.clone.1..sunk, s32[]{:T(128)} %constant.33.clone.1..sunk, s32[]{:T(128)} %constant.33.clone.1..sunk, s32[]{:T(128)} %constant.33.clone.1..sunk) | dynamic-update-slice | bytes 131076 | tf_op jit(solution)/shard_map/while/body/jit(dynamic_update_index_in_dim)/dynamic_update_slice | solution.py:171
  156.3 2.8 %dynamic_update_slice.6 = f32[4,64,1,4,64]{1,0,4,3,2:T(4,128)S(1)} dynamic-update-slice(f32[4,64,1,4,64]{1,0,4,3,2:T(4,128)S(1)} %get-tuple-element.209, f32[1,64,1,4,64]{1,0,4,3,2:T(1,128)S(1)} %bitcast.295, s32[]{:T(128)} %get-tuple-element.207, s32[]{:T(128)} %constant.33.clone.1..sunk, s32[]{:T(128)} %constant.33.clone.1..sunk, s32[]{:T(128)} %constant.33.clone.1..sunk, s32[]{:T(128)} %constant.33.clone.1..sunk) | dynamic-update-slice | bytes 131076 | tf_op jit(solution)/shard_map/while/body/jit(dynamic_update_index_in_dim)/dynamic_update_slice | solution.py:171
  159.8 12.4 %all-gather = bf16[4,4,64,128]{3,2,1,0:T(8,128)(2,1)S(1)} all-gather(bf16[1,4,64,128]{3,2,1,0:T(8,128)(2,1)S(1)} %convert_element_type.353), channel_id=2, replica_groups=mesh['ep_0'=8,'ep_1'=4,'tp_0'=8,'tp_1'=2] {'ep_1'}, dimensions={0}, use_global_device_ids=true | all-gather | bytes 327680 | tf_op jit(solution)/shard_map/all_gather | solution.py:37
  172.3 25.3 %all_gather.22 = bf16[8,1,4,64,128]{4,3,2,1,0:T(8,128)(2,1)S(1)} all-gather(bf16[1,1,4,64,128]{4,3,2,1,0:T(8,128)(2,1)S(1)} %fusion.116), channel_id=1, replica_groups=mesh['ep_0'=8,'ep_1'=4,'tp_0'=8,'tp_1'=2] {'ep_0'}, dimensions={0}, use_global_device_ids=true | all-gather | bytes 589824 | tf_op jit(solution)/shard_map/all_gather | solution.py:37
  199.8 7.0 %all-to-all-start = ((bf16[16,16,2048]{2,1,0:T(8,128)(2,1)}), bf16[16,16,2048]{2,1,0:T(8,128)(2,1)}, u32[]{:S(2)}, u32[]{:S(2)}) async-start(bf16[16,16,2048]{2,1,0:T(8,128)(2,1)} %bitcast.49), calls=%async_computation | async-start | bytes 2097152 | tf_op jit(solution)/shard_map/all_to_all | solution.py:59
  206.9 3.8 %copy.143 = bf16[32,1,24,256]{2,0,1,3:T(8,128)(2,1)S(1)} copy(bf16[32,1,24,256]{3,2,0,1:T(8,128)(2,1)} %reduce-scatter.5.cloned.1.call-done) | data formatting | bytes 786432
  210.7 4.2 %reshape.651 = bf16[256,768]{1,0:T(8,128)(2,1)} reshape(bf16[256,1,32,24]{3,2,1,0:T(8,128)(2,1)S(1)} %bitcast.297) | data formatting | bytes 786432
  215.0 11.6 %reduce-scatter.7.cloned.1.call-done = bf16[128,768]{1,0:T(8,128)(2,1)} async-done(((bf16[256,768]{1,0:T(8,128)(2,1)}), bf16[128,768]{1,0:T(8,128)(2,1)}) %reduce-scatter.7.cloned.1.call-update) | async-done | bytes 196624
  231.6 9.6 %all-to-all-start.3 = ((bf16[32,1,24,128]{3,2,1,0:T(8,128)(2,1)}), bf16[32,1,24,128]{3,2,1,0:T(8,128)(2,1)S(1)}, u32[]{:S(2)}, u32[]{:S(2)}) async-start(bf16[32,1,24,128]{3,2,1,0:T(8,128)(2,1)} %bitcast.73), calls=%async_computation.4 | async-start | bytes 393216 | tf_op jit(solution)/shard_map/all_to_all | solution.py:266
  243.2 10.1 %all-to-all-done.3 = bf16[32,1,24,128]{3,2,1,0:T(8,128)(2,1)S(1)} async-done(((bf16[32,1,24,128]{3,2,1,0:T(8,128)(2,1)}), bf16[32,1,24,128]{3,2,1,0:T(8,128)(2,1)S(1)}, u32[]{:S(2)}, u32[]{:S(2)}) %all-to-all-start.3) | async-done | bytes 196640 | tf_op jit(solution)/shard_map/all_to_all | solution.py:266
  (165 shorter events, 31.4 us)
Async XLA Ops:
  7.2 127.9 %copy-start = (bf16[1,256,2048]{2,1,0:T(8,128)(2,1)S(1)}, bf16[1,256,2048]{2,1,0:T(8,128)(2,1)}, u32[]{:S(2)}) copy-start(bf16[1,256,2048]{2,1,0:T(8,128)(2,1)} %param.41) | copy-start | bytes 3145732
  41.3 7.8 %copy-start.2 = (bf16[256,256]{1,0:T(8,128)(2,1)S(1)}, bf16[256,256]{1,0:T(8,128)(2,1)}, u32[]{:S(2)}) copy-start(bf16[256,256]{1,0:T(8,128)(2,1)} %param.23) | copy-start | bytes 393220
  41.3 9.7 %copy-start.4 = (bf16[256,128]{1,0:T(8,128)(2,1)S(1)}, bf16[256,128]{1,0:T(8,128)(2,1)}, u32[]{:S(2)}) copy-start(bf16[256,128]{1,0:T(8,128)(2,1)} %param.25) | copy-start | bytes 196612
  41.3 13.1 %copy-start.14 = (f32[4]{0:T(128)S(1)}, f32[4]{0:T(128)}, u32[]{:S(2)}) copy-start(f32[4]{0:T(128)} %param.33) | copy-start | bytes 52
  41.3 13.2 %copy-start.7 = (f32[256,4]{0,1:T(4,128)S(1)}, f32[256,4]{0,1:T(4,128)}, u32[]{:S(2)}) copy-start(f32[256,4]{0,1:T(4,128)} %param.28) | copy-start | bytes 12292
  41.3 13.2 %copy-start.8 = (f32[256,4]{0,1:T(4,128)S(1)}, f32[256,4]{0,1:T(4,128)}, u32[]{:S(2)}) copy-start(f32[256,4]{0,1:T(4,128)} %param.27) | copy-start | bytes 12292
  41.3 13.2 %copy-start.12 = (f32[4]{0:T(128)S(1)}, f32[4]{0:T(128)}, u32[]{:S(2)}) copy-start(f32[4]{0:T(128)} %param.32) | copy-start | bytes 52
  41.3 14.7 %copy-start.5 = (bf16[256,128]{1,0:T(8,128)(2,1)S(1)}, bf16[256,128]{1,0:T(8,128)(2,1)}, u32[]{:S(2)}) copy-start(bf16[256,128]{1,0:T(8,128)(2,1)} %param.24) | copy-start | bytes 196612
  41.3 42.0 %copy-start.10 = (bf16[4,128]{1,0:T(4,128)(2,1)S(1)}, bf16[4,128]{1,0:T(4,128)(2,1)}, u32[]{:S(2)}) copy-start(bf16[4,128]{1,0:T(4,128)(2,1)} %param.31) | copy-start | bytes 3076
  41.3 42.0 %copy-start.11 = (bf16[4,128]{1,0:T(4,128)(2,1)S(1)}, bf16[4,128]{1,0:T(4,128)(2,1)}, u32[]{:S(2)}) copy-start(bf16[4,128]{1,0:T(4,128)(2,1)} %param.30) | copy-start | bytes 3076
  41.3 42.1 %copy-start.6 = (bf16[4,256]{1,0:T(4,128)(2,1)S(1)}, bf16[4,256]{1,0:T(4,128)(2,1)}, u32[]{:S(2)}) copy-start(bf16[4,256]{1,0:T(4,128)(2,1)} %param.29) | copy-start | bytes 6148
  41.3 42.3 %copy-start.15 = (bf16[256]{0:T(256)(128)(2,1)S(1)}, bf16[256]{0:T(256)(128)(2,1)}, u32[]{:S(2)}) copy-start(bf16[256]{0:T(256)(128)(2,1)} %param.35) | copy-start | bytes 1540
  41.4 77.5 %all-to-all-start.2 = ((bf16[16,32,1,24,128]{4,3,1,2,0:T(8,128)(2,1)}), bf16[16,32,1,24,128]{4,3,1,2,0:T(8,128)(2,1)}, u32[]{:S(2)}, u32[]{:S(2)}) async-start(bf16[16,32,1,24,128]{4,3,1,2,0:T(8,128)(2,1)} %stack.2), calls=%async_computation.2 | async-start | bytes 6291456 | tf_op jit(solution)/shard_map/all_to_all | solution.py:243
  49.1 157.8 %reduce-scatter.5.cloned.1.call-start = ((), (), s32[]{:S(2)}) async-start(), calls=%async_computation.6 | async-start | bytes 3538944 | tf_op jit(solution)/shard_map/reduce_scatter | solution.py:65
  49.1 34.8 %collective-permute-start = (bf16[3,256]{1,0:T(4,128)(2,1)S(1)}, bf16[3,256]{1,0:T(4,128)(2,1)S(1)}, u32[]{:S(2)}, u32[]{:S(2)}) collective-permute-start(bf16[3,256]{1,0:T(4,128)(2,1)S(1)} %slice.180), channel_id=1, source_target_pairs={{0,16},{16,32},{32,48},{48,64},{64,80},{80,96},{96,112},{112,128},... | collective-permute-start | bytes 4616 | tf_op jit(solution)/shard_map/ppermute | solution.py:22
  51.0 32.6 %collective-permute-start.2 = (bf16[3,128]{1,0:T(4,128)(2,1)S(1)}, bf16[3,128]{1,0:T(4,128)(2,1)S(1)}, u32[]{:S(2)}, u32[]{:S(2)}) collective-permute-start(bf16[3,128]{1,0:T(4,128)(2,1)S(1)} %slice.198), channel_id=1, source_target_pairs={{0,16},{16,32},{32,48},{48,64},{64,80},{80,96},{96,112},{112,128},... | collective-permute-start | bytes 2312 | tf_op jit(solution)/shard_map/ppermute | solution.py:22
  56.4 27.3 %collective-permute-start.1 = (bf16[3,128]{1,0:T(4,128)(2,1)S(1)}, bf16[3,128]{1,0:T(4,128)(2,1)S(1)}, u32[]{:S(2)}, u32[]{:S(2)}) collective-permute-start(bf16[3,128]{1,0:T(4,128)(2,1)S(1)} %slice.189), channel_id=1, source_target_pairs={{0,16},{16,32},{32,48},{48,64},{64,80},{80,96},{96,112},{112,128},... | collective-permute-start | bytes 2312 | tf_op jit(solution)/shard_map/ppermute | solution.py:22
  143.3 54.3 %copy-start.16 = (f32[4]{0:T(128)S(1)}, f32[4]{0:T(128)}, u32[]{:S(2)}) copy-start(f32[4]{0:T(128)} %param.34) | copy-start | bytes 52
  159.3 38.9 %copy-start.3 = (bf16[256,256]{1,0:T(8,128)(2,1)S(1)}, bf16[256,256]{1,0:T(8,128)(2,1)}, u32[]{:S(2)}) copy-start(bf16[256,256]{1,0:T(8,128)(2,1)} %param.26) | copy-start | bytes 393220
  159.8 38.5 %copy-start.13 = (bf16[256,2048]{1,0:T(8,128)(2,1)S(1)}, bf16[256,2048]{1,0:T(8,128)(2,1)}, u32[]{:S(2)}) copy-start(bf16[256,2048]{1,0:T(8,128)(2,1)} %param.36) | copy-start | bytes 3145732
  199.8 31.8 %all-to-all-start = ((bf16[16,16,2048]{2,1,0:T(8,128)(2,1)}), bf16[16,16,2048]{2,1,0:T(8,128)(2,1)}, u32[]{:S(2)}, u32[]{:S(2)}) async-start(bf16[16,16,2048]{2,1,0:T(8,128)(2,1)} %bitcast.49), calls=%async_computation | async-start | bytes 2097152 | tf_op jit(solution)/shard_map/all_to_all | solution.py:59
  206.8 19.7 %reduce-scatter.7.cloned.1.call-start = ((), (), s32[]{:S(2)}) async-start(), calls=%async_computation.7 | async-start | bytes 589824
  210.7 30.4 %copy-start.9 = (f32[256,2]{0,1:T(2,128)S(1)}, f32[256,2]{0,1:T(2,128)}, u32[]{:S(2)}) copy-start(f32[256,2]{0,1:T(2,128)} %param.43) | copy-start | bytes 6148
  231.6 21.8 %all-to-all-start.3 = ((bf16[32,1,24,128]{3,2,1,0:T(8,128)(2,1)}), bf16[32,1,24,128]{3,2,1,0:T(8,128)(2,1)S(1)}, u32[]{:S(2)}, u32[]{:S(2)}) async-start(bf16[32,1,24,128]{3,2,1,0:T(8,128)(2,1)} %bitcast.73), calls=%async_computation.4 | async-start | bytes 393216 | tf_op jit(solution)/shard_map/all_to_all | solution.py:266
  (1 other events, 1.0 us)
Sparse Core Ops, SparseCore 0:
  142.4 43.1 reduce-scatter.4
  215.1 11.4 reduce-scatter.6
